TPU v7x, 32 devices: a whole 2x2x4 slice. The times are simulated.
32 devices in a mesh: kv: 8 (over z, x), tp: 4 (over y, core).
Axes of the slice: x: 2, y: 2, z: 4, core: 2. Of those that a mesh axis runs over, the one named last changes fastest.
Arguments:
- tokens: bfloat16 [4096, 2048], P('kv'), may hold values from -64 to 64
- query_weight: bfloat16 [2048, 2048], P(None, 'tp'), may hold values from -0.1875 to 0.1875
- chosen_key_weight: bfloat16 [2048, 512], P(None, 'tp'), may hold values from -0.125 to 0.125
- chosen_value_weight: bfloat16 [2048, 512], P(None, 'tp'), may hold values from -0.125 to 0.125
- summary_key_weight: bfloat16 [2048, 512], P(None, 'tp'), may hold values from -0.125 to 0.125
- summary_value_weight: bfloat16 [2048, 512], P(None, 'tp'), may hold values from -0.125 to 0.125
- squeeze_key_in: bfloat16 [2048, 128], replicated, may hold values from -0.125 to 0.125
- squeeze_key_out: bfloat16 [128, 64], replicated, may hold values from -1 to 1
- squeeze_value_in: bfloat16 [2048, 128], replicated, may hold values from -0.125 to 0.125
- squeeze_value_out: bfloat16 [128, 64], replicated, may hold values from -2 to 2
- gate_weight: bfloat16 [2, 2048, 32], P(None, None, 'tp'), may hold values from -0.125 to 0.125
- output_weight: bfloat16 [2048, 2048], P('tp'), may hold values from -1 to 1
- chosen_blocks: int32 [8, 128, 16], P('tp', 'kv'), may hold values from 0 to 127, as said below
Outputs:
- attended: bfloat16 [4096, 2048], P(('kv', 'tp'))
Inputs may be any that keep to these rules, and one draw needn't show every extreme that they name: `chosen_blocks`: each row lists 16 different blocks. The row of query block b lists b, lists b - 1 where b > 0, and lists block 0. Take the blocks at or below their query block that the rows of the query blocks of one index of kv list for one key head: at most 4 different ones lie among the positions of any other single index of kv, and exactly 4 among the positions of the first index, for every index after the first.
All inputs are finite; a program needn't handle non-finite values.
Results may differ from a plain program's by a relative error of at most 0.03.
Values may be sent and summed in bfloat16 or wider, within the bound.
A program may use at most 128 MiB of HBM per device.

v0:
```python
import jax
import jax.numpy as jnp
from jax import lax
from jax.sharding import PartitionSpec as P

HD = 64
CMP_LEN = 32
CMP_STRIDE = 16
BLK = 32
ROTARY_BASE = 10000.0
NEGATIVE_FILL = -1e30


def from_behind(block, axis, distance):
    devices = range(lax.axis_size(axis))
    route = [(i - distance, i) for i in devices if i - distance in devices]
    return lax.ppermute(block, axis, route)


def rotate(values, positions):
    halfway = values.shape[-1] // 2
    inverse = ROTARY_BASE ** (-jnp.arange(halfway, dtype=jnp.float32) / halfway)
    angles = positions.astype(jnp.float32)[:, None] * inverse[None, :]
    cosine_rows = jnp.cos(angles)[:, None, :]
    sine_rows = jnp.sin(angles)[:, None, :]
    former = values[..., :halfway]
    latter = values[..., halfway:]
    return jnp.concatenate(
        [former * cosine_rows - latter * sine_rows, latter * cosine_rows + former * sine_rows], -1
    )


def squeeze_windows(windows, weight_in, weight_out):
    total_windows = windows.shape[0]
    groups = windows.shape[2]
    head_width = windows.shape[3]
    flattened = windows.transpose(0, 2, 1, 3).reshape(total_windows * groups, CMP_LEN * head_width)
    hidden = jax.nn.gelu(jnp.dot(flattened, weight_in, preferred_element_type=jnp.float32)).astype(
        jnp.bfloat16
    )
    return jnp.dot(hidden, weight_out, preferred_element_type=jnp.float32).reshape(
        total_windows, groups, head_width
    )


def online_step(running, scores, visible, values):
    largest, summed, weighted = running
    updated = jnp.maximum(largest, jnp.max(jnp.where(visible, scores, NEGATIVE_FILL), -1))
    weights = jnp.where(visible, jnp.exp(scores - updated[..., None]), 0.0)
    shrink = jnp.exp(largest - updated)
    summed = summed * shrink + jnp.sum(weights, -1)
    weighted = weighted * shrink[..., None] + jnp.einsum(
        "grqk,kgd->grqd", weights.astype(jnp.bfloat16), values, preferred_element_type=jnp.float32
    )
    return (updated, summed, weighted)


def on_device(
    tokens,
    query_weight,
    chosen_key_weight,
    chosen_value_weight,
    summary_key_weight,
    summary_value_weight,
    squeeze_key_in,
    squeeze_key_out,
    squeeze_value_in,
    squeeze_value_out,
    gate_weight,
    output_weight,
    chosen_blocks,
):
    tok_rows = tokens.shape[0]
    heads_here = query_weight.shape[1] // HD
    groups_here = chosen_key_weight.shape[1] // HD
    per_group = heads_here // groups_here
    kv_rank = lax.axis_index("kv")
    offset = kv_rank * tok_rows
    positions = offset + jnp.arange(tok_rows, dtype=jnp.int32)
    queries = rotate(
        jnp.dot(tokens, query_weight, preferred_element_type=jnp.float32).reshape(
            tok_rows, heads_here, HD
        ),
        positions,
    )
    queries = queries.astype(jnp.bfloat16).reshape(tok_rows, groups_here, per_group, HD)
    chosen_keys = rotate(
        jnp.dot(tokens, chosen_key_weight, preferred_element_type=jnp.float32).reshape(
            tok_rows, groups_here, HD
        ),
        positions,
    ).astype(jnp.bfloat16)
    chosen_values = (
        jnp.dot(tokens, chosen_value_weight, preferred_element_type=jnp.float32)
        .astype(jnp.bfloat16)
        .reshape(tok_rows, groups_here, HD)
    )
    chosen_pairs = jnp.concatenate([chosen_keys, chosen_values], -1)
    raw_keys = (
        jnp.dot(tokens, summary_key_weight, preferred_element_type=jnp.float32)
        .astype(jnp.bfloat16)
        .reshape(tok_rows, groups_here, HD)
    )
    raw_values = (
        jnp.dot(tokens, summary_value_weight, preferred_element_type=jnp.float32)
        .astype(jnp.bfloat16)
        .reshape(tok_rows, groups_here, HD)
    )
    raw_pairs = jnp.concatenate([raw_keys, raw_values], -1)
    following = from_behind(raw_pairs[:CMP_STRIDE], "kv", -1)
    extended = jnp.concatenate([raw_pairs, following], 0)
    summary_count = tok_rows // CMP_STRIDE
    segments = extended.reshape(summary_count + 1, CMP_STRIDE, groups_here, 2 * HD)
    windows = jnp.concatenate([segments[:-1], segments[1:]], 1)
    summary_ends = (
        (kv_rank * summary_count + jnp.arange(summary_count, dtype=jnp.int32)) * CMP_STRIDE
        + CMP_LEN
        - 1
    )
    summary_keys = rotate(
        squeeze_windows(windows[..., :HD], squeeze_key_in, squeeze_key_out), summary_ends
    ).astype(jnp.bfloat16)
    summary_values = squeeze_windows(windows[..., HD:], squeeze_value_in, squeeze_value_out).astype(
        jnp.bfloat16
    )
    summaries = jnp.concatenate([summary_keys, summary_values], -1)
    scaling = HD ** (-0.5)
    starting = (
        jnp.full((groups_here, per_group, tok_rows), NEGATIVE_FILL, jnp.float32),
        jnp.zeros((groups_here, per_group, tok_rows), jnp.float32),
        jnp.zeros((groups_here, per_group, tok_rows, HD), jnp.float32),
    )
    portion = lax.all_gather(summaries, "kv", axis=0, tiled=True)
    length = portion.shape[0]
    ends = jnp.arange(length, dtype=jnp.int32) * CMP_STRIDE + CMP_LEN - 1
    scores = (
        jnp.einsum("qgrd,kgd->grqk", queries, portion[..., :HD], preferred_element_type=jnp.float32)
        * scaling
    )
    visible = (ends[None, :] <= positions[:, None])[None, None]
    folded = online_step(starting, scores, visible, portion[..., HD:])
    compressed = folded[2] / jnp.maximum(folded[1], 1.0)[..., None]
    block_count = tok_rows // BLK

    def span_step(running, stretch, leading):
        length = stretch.shape[0]
        key_positions = leading + jnp.arange(length, dtype=jnp.int32)
        listed = jnp.any(
            chosen_blocks[:, :, :, None] == (key_positions // BLK)[None, None, None, :], axis=2
        )
        listed = jnp.broadcast_to(
            listed[:, :, None, :], (groups_here, block_count, BLK, length)
        ).reshape(groups_here, tok_rows, length)
        visible = (listed & (key_positions[None, None, :] <= positions[None, :, None]))[:, None]
        scores = (
            jnp.einsum(
                "qgrd,kgd->grqk", queries, stretch[..., :HD], preferred_element_type=jnp.float32
            )
            * scaling
        )
        return online_step(running, scores, visible, stretch[..., HD:])

    def maybe_step(running, stretch, leading):

        def step_taken(carried):
            return span_step(carried, stretch, leading)

        def step_skipped(carried):
            return carried

        return lax.cond(leading <= offset + tok_rows - 1, step_taken, step_skipped, running)

    portion = lax.all_gather(chosen_pairs, "kv", axis=0, tiled=True)
    length = portion.shape[0]
    stretch_rows = tok_rows * 4

    def visit_span(number, carried):
        stretch = lax.dynamic_slice_in_dim(portion, number * stretch_rows, stretch_rows, 0)
        return maybe_step(carried, stretch, number * stretch_rows)

    folded_chosen = lax.fori_loop(0, length // stretch_rows, visit_span, starting)
    selected = folded_chosen[2] / folded_chosen[1][..., None]
    first_gates = jax.nn.sigmoid(
        jnp.dot(tokens, gate_weight[0], preferred_element_type=jnp.float32)
    )
    second_gates = jax.nn.sigmoid(
        jnp.dot(tokens, gate_weight[1], preferred_element_type=jnp.float32)
    )
    first_gates = first_gates.reshape(tok_rows, groups_here, per_group).transpose(1, 2, 0)[
        ..., None
    ]
    second_gates = second_gates.reshape(tok_rows, groups_here, per_group).transpose(1, 2, 0)[
        ..., None
    ]
    blended = (
        (first_gates * compressed + second_gates * selected)
        .transpose(2, 0, 1, 3)
        .reshape(tok_rows, heads_here * HD)
        .astype(jnp.bfloat16)
    )
    attended = lax.psum_scatter(
        jnp.dot(blended, output_weight, preferred_element_type=jnp.float32).astype(jnp.bfloat16),
        "tp",
        scatter_dimension=0,
        tiled=True,
    )
    return attended


def solution(mesh):
    return jax.shard_map(
        on_device,
        mesh=mesh,
        in_specs=(
            P("kv", None),
            P(None, "tp"),
            P(None, "tp"),
            P(None, "tp"),
            P(None, "tp"),
            P(None, "tp"),
            P(),
            P(),
            P(),
            P(),
            P(None, None, "tp"),
            P("tp", None),
            P("tp", "kv", None),
        ),
        out_specs=P(("kv", "tp"), None),
        check_vma=False,
    )
```

profile of v0, /device:TPU:0, one launch (start us, length us, event | category | flops | bytes accessed | tf_op | source)
XLA Modules:
  0.0 240.7 jit_solution(17851520680205878891)
XLA Ops:
  6.6 2.7 %convolution_convert_fusion.1 = bf16[512,128]{0,1:T(8,128)(2,1)S(1)} fusion(bf16[512,2048]{1,0:T(8,128)(2,1)} %param.17, bf16[2048,128]{1,0:T(8,128)(2,1)} %param.20), kind=kOutput, calls=%fused_computation.44 | convolution fusion | flops 268500992 | bytes 2752512 | tf_op jit(solution)/shard_map/dot_general | solution.py:94
  9.2 2.5 %fusion.91 = f32[512,128]{0,1:T(8,128)S(1)} fusion(bf16[512,2048]{1,0:T(8,128)(2,1)} %param.17, bf16[2048,128]{1,0:T(8,128)(2,1)} %param.19), kind=kOutput, calls=%fused_computation.133 | convolution fusion | flops 268435456 | bytes 2883584 | tf_op jit(solution)/shard_map/dot_general | solution.py:88
  12.9 2.4 %convolution_convert_fusion.2 = bf16[512,128]{0,1:T(8,128)(2,1)S(1)} fusion(bf16[512,2048]{1,0:T(8,128)(2,1)} %param.17, bf16[2048,128]{1,0:T(8,128)(2,1)S(1)} %copy-done.7), kind=kOutput, calls=%fused_computation.45 | convolution fusion | flops 268500992 | bytes 2752512 | tf_op jit(solution)/shard_map/dot_general | solution.py:105
  15.5 2.5 %convolution_convert_fusion.3 = bf16[512,128]{0,1:T(8,128)(2,1)S(1)} fusion(bf16[512,2048]{1,0:T(8,128)(2,1)} %param.17, bf16[2048,128]{1,0:T(8,128)(2,1)} %param.21), kind=kOutput, calls=%fused_computation.46 | convolution fusion | flops 268500992 | bytes 2752512 | tf_op jit(solution)/shard_map/dot_general | solution.py:100
  18.9 1.3 collective-permute-start
  20.2 3.5 %fusion.90 = f32[512,512]{0,1:T(8,128)S(1)} fusion(bf16[512,2048]{1,0:T(8,128)(2,1)} %param.17, bf16[2048,512]{1,0:T(8,128)(2,1)} %param.18), kind=kOutput, calls=%fused_computation.132 | convolution fusion | flops 1073741824 | bytes 5242880 | tf_op jit(solution)/shard_map/dot_general | solution.py:81
  24.8 2.9 %fusion.34 = f32[512,8]{0,1:T(8,128)} fusion(bf16[512,2048]{1,0:T(8,128)(2,1)} %param.17, bf16[2,2048,8]{1,2,0:T(8,128)(2,1)} %param.27), kind=kOutput, calls=%fused_computation.51 | convolution fusion | flops 16789504 | bytes 2146304 | tf_op jit(solution)/shard_map/dot_general | solution.py:187
  27.7 2.3 fusion.37
  34.4 1.3 reshape.285
  40.6 1.4 fusion.64
  42.9 1.4 convolution_convert_fusion.4
  44.4 35.0 %all_gather.6 = bf16[256,2,128]{2,1,0:T(2,128)(2,1)S(1)} all-gather(bf16[32,2,128]{2,1,0:T(2,128)(2,1)S(1)} %pad_maximum_fusion.5), channel_id=1, replica_groups=mesh['kv'=8,'tp'=4] {'kv'}, dimensions={0}, use_global_device_ids=true | all-gather | bytes 147456 | tf_op jit(solution)/shard_map/all_gather | solution.py:133
  80.5 1.9 fusion.21
  82.4 2.0 copy-done.2
  86.2 55.0 %while.20 = (s32[]{:T(128)}, f32[2,4,512]{2,1,0:T(4,128)S(1)}, f32[2,4,512]{2,1,0:T(4,128)S(1)}, f32[2,4,512,64]{2,3,1,0:T(8,128)S(1)}, s32[]{:T(128)}, /*index=...) while((s32[]{:T(128)}, f32[2,4,512]{2,1,0:T(4,128)S(1)}, ...), condition=%wide.region_8.9_spmd.clone, body=%wide.region_2.8_spmd.clone.sunk | while | flops 2245501440 | bytes 127838584 | solution.py:181
  86.2 54.9 %conditional.3 = ((f32[2,4,512]{2,1,0:T(4,128)S(1)}, f32[2,4,512]{2,1,0:T(4,128)S(1)}, f32[2,4,512,64]{2,3,1,0:T(8,128)S(1)})) conditional(s32[]{:T(128)} %convert_element_type.107, (f32[2,4,512]{2,1,0:T(4,128)S(1)}, f32[2,4,512]{2,1,0:T(4,128)S(1)}, f32[2,4,512,64]{2,3,1,0:T(8,128)S(1)}) %tuple.69, (s32[2,16,16]{2,1,0:T(8,128)S(1)}, s32[]{:T(128)}, ...), branch_computations={%region_3.3_spmd, %region_4.7_spmd} | conditional | flops 2245501440 | bytes 127836296 | solution.py:171
  88.0 2.6 %bitcast_and_fusion = pred[2,512,2048]{2,1,0:T(8,128)(4,1)} fusion(pred[512,2048]{1,0:T(8,128)(4,1)S(1)} %broadcast_compare_fusion, pred[2,16,2048]{2,1,0:T(8,128)(4,1)S(1)} %compare_reduce_fusion), kind=kLoop, calls=%fused_computation.10 | loop fusion | flops 2097152 | bytes 3211264 | tf_op jit(solution)/shard_map/while/body/eval_jaxpr/cond/branch_1_fun/and | solution.py:154
  90.6 6.1 %copy.48 = pred[2,512,2048]{1,2,0:T(8,128)(4,1)} copy(pred[2,512,2048]{2,1,0:T(8,128)(4,1)} %bitcast_and_fusion) | data formatting | bytes 4194304 | tf_op jit(solution)/shard_map/while/body/eval_jaxpr/cond/branch_1_fun/and | solution.py:154
  96.6 15.2 %fusion.2 = (f32[2,4,512]{2,1,0:T(4,128)S(1)}, f32[2,2048,512,4]{2,1,3,0:T(8,128)}) fusion(pred[2,512,2048]{1,2,0:T(8,128)(4,1)} %copy.48, bf16[512,2,4,64]{0,3,2,1:T(8,128)(2,1)} %get-tuple-element.301, bf16[4096,2,128]{0,2,1:T(8,128)(2,1)} %get-tuple-element.300, s32[]{:T(128)S(6)} %select_n.35), kind=kOutput, calls=%fused_computation.3 | convolution fusion | flops 1098903552 | bytes 36716548 | tf_op jit(solution)/shard_map/while/body/eval_jaxpr/cond/branch_1_fun/qgrd,kgd->grqk/dot_general | solution.py:156
  111.9 14.3 %fusion.6 = f32[2,4,512]{2,1,0:T(4,128)S(1)} fusion(f32[2,2048,512,4]{2,1,3,0:T(8,128)} %get-tuple-element.369, f32[2,4,512]{2,1,0:T(4,128)S(1)} %max.12, pred[2,512,2048]{1,2,0:T(8,128)(4,1)S(1)} %copy-done.1), kind=kLoop, calls=%fused_computation.7 | loop fusion | flops 33550336 | bytes 35684352 | tf_op jit(solution)/shard_map/while/body/eval_jaxpr/cond/branch_1_fun/reduce_sum | solution.py:51
  126.2 14.9 %fusion.10 = f32[2,4,512,64]{2,3,1,0:T(8,128)S(1)} fusion(f32[2,2048,512,4]{2,1,3,0:T(8,128)} %get-tuple-element.369, f32[2,4,512]{2,1,0:T(4,128)S(1)} %max.12, pred[2,512,2048]{1,2,0:T(8,128)(4,1)} %copy.48, f32[2,4,512,64]{2,3,1,0:T(8,128)S(1)} %get-tuple-element.303, bf16[4096,2,128]{0,2,1:T(8,128)(2,1)} %get-tuple-element.300, s32[]{:T(128)S(6)} %select_n.35, ...), kind=kOutput, calls=%fused_computation.13 | convolution fusion | flops 1107820544 | bytes 38305800 | tf_op jit(solution)/shard_map/while/body/eval_jaxpr/cond/branch_1_fun/grqk,kgd->grqd/dot_general | solution.py:52
  141.3 3.3 %add_convert_fusion = bf16[2,4,512,64]{2,3,1,0:T(8,128)(2,1)S(1)} fusion(f32[2,4,512,64]{2,3,1,0:T(8,128)S(1)} %get-tuple-element.319, f32[2,256,512,4]{2,1,3,0:T(8,128)} %copy-done.2, f32[2,4,512]{2,1,0:T(4,128)} %copy-done.9, pred[512,256]{0,1:T(8,128)(4,1)S(1)} %copy-done.6, f32[2,4,512]{2,1,0:T(4,128)S(1)} %get-tuple-element.320, ...), kind=kOutput, calls=%fused_computation.56 | convolution fusion | flops 140247040 | bytes 6062080 | tf_op jit(solution)/shard_map/grqk,kgd->grqd/dot_general | solution.py:52
  144.5 2.6 %convolution_convert_fusion = bf16[512,2048]{1,0:T(8,128)(2,1)} fusion(bf16[512,512]{0,1:T(8,128)(2,1)S(1)} %bitcast.140, bf16[512,2048]{1,0:T(8,128)(2,1)S(1)} %copy-done), kind=kOutput, calls=%fused_computation.40 | convolution fusion | flops 1074790400 | bytes 4718592 | tf_op jit(solution)/shard_map/dot_general | solution.py:202
  147.2 86.7 %reduce-scatter.2.cloned.1.call-done = bf16[128,2048]{1,0:T(8,128)(2,1)} async-done(((bf16[512,2048]{1,0:T(8,128)(2,1)}), bf16[128,2048]{1,0:T(8,128)(2,1)}) %reduce-scatter.2.cloned.1.call-update) | async-done | bytes 524304 | tf_op jit(solution)/shard_map/reduce_scatter | solution.py:201
  (86 shorter events, 18.0 us)
Async XLA Ops:
  6.5 138.0 %copy-start = (bf16[512,2048]{1,0:T(8,128)(2,1)S(1)}, bf16[512,2048]{1,0:T(8,128)(2,1)}, u32[]{:S(2)}) copy-start(bf16[512,2048]{1,0:T(8,128)(2,1)} %param.28) | copy-start | bytes 6291460
  6.5 6.4 %copy-start.7 = (bf16[2048,128]{1,0:T(8,128)(2,1)S(1)}, bf16[2048,128]{1,0:T(8,128)(2,1)}, u32[]{:S(2)}) copy-start(bf16[2048,128]{1,0:T(8,128)(2,1)} %param.22) | copy-start | bytes 1572868
  6.5 79.4 %all-gather.2.cloned.1.call-start = ((), (), s32[]{:S(2)}) async-start(), calls=%async_computation.1 | async-start | bytes 2359296 | tf_op jit(solution)/shard_map/all_gather | solution.py:173
  12.8 221.0 %reduce-scatter.2.cloned.1.call-start = ((), (), s32[]{:S(2)}) async-start(), calls=%async_computation.2 | async-start | bytes 2621440 | tf_op jit(solution)/shard_map/reduce_scatter | solution.py:201
  18.9 17.5 %collective-permute-start = (bf16[16,2,128]{2,0,1:T(8,128)(2,1)}, bf16[16,2,128]{2,0,1:T(8,128)(2,1)}, u32[]{:S(2)}, u32[]{:S(2)}) collective-permute-start(bf16[16,2,128]{2,0,1:T(8,128)(2,1)} %pad_maximum_fusion.6), channel_id=1, source_target_pairs={{4,0},{8,4},{12,8},{16,12},{20,16},{24,20},{28,24},{5,1},{9,5},{13... | collective-permute-start | bytes 24584 | tf_op jit(solution)/shard_map/ppermute | solution.py:17
  23.9 8.4 %copy-start.3 = (bf16[512,8,32]{0,2,1:T(8,128)(2,1)}, bf16[512,8,32]{0,2,1:T(8,128)(2,1)S(1)}, u32[]{:S(2)}) copy-start(bf16[512,8,32]{0,2,1:T(8,128)(2,1)S(1)} %get-tuple-element.372) | copy-start | bytes 786436
  23.9 14.6 %copy-start.4 = (bf16[512,8,32]{0,2,1:T(8,128)(2,1)}, bf16[512,8,32]{0,2,1:T(8,128)(2,1)S(1)}, u32[]{:S(2)}) copy-start(bf16[512,8,32]{0,2,1:T(8,128)(2,1)S(1)} %get-tuple-element.373) | copy-start | bytes 786436
  24.0 58.4 %copy-start.5 = (pred[512,256]{0,1:T(8,128)(4,1)}, pred[512,256]{0,1:T(8,128)(4,1)S(1)}, u32[]{:S(2)}) copy-start(pred[512,256]{0,1:T(8,128)(4,1)S(1)} %broadcast_compare_fusion.1) | copy-start | bytes 393220
  37.2 4.9 %copy-start.11 = (f32[32,32]{1,0:T(8,128)S(1)}, f32[32,32]{1,0:T(8,128)}, u32[]{:S(2)}) copy-start(f32[32,32]{1,0:T(8,128)} %get-tuple-element.386) | copy-start | bytes 12292
  80.5 5.6 %copy-start.8 = (s32[2,16,16]{2,1,0:T(8,128)S(1)}, s32[2,16,16]{2,1,0:T(8,128)}, u32[]{:S(2)}) copy-start(s32[2,16,16]{2,1,0:T(8,128)} %param.29) | copy-start | bytes 6148
  82.4 2.1 copy-start.2
  82.4 3.8 %copy-start.9 = (f32[2,4,512]{2,1,0:T(4,128)}, f32[2,4,512]{2,1,0:T(4,128)S(1)}, u32[]{:S(2)}) copy-start(f32[2,4,512]{2,1,0:T(4,128)S(1)} %broadcast_maximum_fusion) | copy-start | bytes 49156
  86.1 55.1 %copy-start.6 = (pred[512,256]{0,1:T(8,128)(4,1)S(1)}, pred[512,256]{0,1:T(8,128)(4,1)}, u32[]{:S(2)}) copy-start(pred[512,256]{0,1:T(8,128)(4,1)} %copy-done.5) | copy-start | bytes 393220
  86.1 55.1 %copy-start.10 = (bf16[256,2,64]{0,2,1:T(8,128)(2,1)S(1)}, bf16[256,2,64]{0,2,1:T(8,128)(2,1)}, u32[]{:S(2)}) copy-start(bf16[256,2,64]{0,2,1:T(8,128)(2,1)} %copy.67) | copy-start | bytes 196612
  86.1 55.1 %copy-start.12 = (f32[512,2,4]{0,2,1:T(4,128)S(1)}, f32[512,2,4]{0,2,1:T(4,128)}, u32[]{:S(2)}) copy-start(f32[512,2,4]{0,2,1:T(4,128)} %reshape.285) | copy-start | bytes 49156
  86.1 55.1 %copy-start.13 = (f32[512,2,4]{0,2,1:T(4,128)S(1)}, f32[512,2,4]{0,2,1:T(4,128)}, u32[]{:S(2)}) copy-start(f32[512,2,4]{0,2,1:T(4,128)} %reshape.278) | copy-start | bytes 49156
  86.2 55.1 %copy-start.14 = (f32[2,4,512]{2,1,0:T(4,128)S(1)}, f32[2,4,512]{2,1,0:T(4,128)}, u32[]{:S(2)}) copy-start(f32[2,4,512]{2,1,0:T(4,128)} %get-tuple-element.382) | copy-start | bytes 49156
  86.2 55.1 %copy-start.15 = (f32[2,4,512]{2,1,0:T(4,128)S(1)}, f32[2,4,512]{2,1,0:T(4,128)}, u32[]{:S(2)}) copy-start(f32[2,4,512]{2,1,0:T(4,128)} %get-tuple-element.383) | copy-start | bytes 49156
  96.6 15.2 %copy-start.1 = (pred[2,512,2048]{1,2,0:T(8,128)(4,1)S(1)}, pred[2,512,2048]{1,2,0:T(8,128)(4,1)}, u32[]{:S(2)}) copy-start(pred[2,512,2048]{1,2,0:T(8,128)(4,1)} %copy.48) | copy-start | bytes 6291460 | tf_op jit(solution)/shard_map/while/body/eval_jaxpr/cond
Sparse Core Ops, SparseCore 0:
  13.0 54.0 all-gather.1
  147.3 86.5 reduce-scatter.1
where the time goes:
time: 242 us; the launch traced here: 241 us
  waiting for transfers between devices  86.8 us (36%)
  matrix products  59.3 us (25%)
  blocking collectives  35 us (14%)
  other arithmetic  26.6 us (11%)
  local copies, waits for them, and re-layouts  17.6 us (7%)
  between operations  13.8 us (6%)
    reduce_scatter x1, waiting for transfers between devices, on_device(): lax.psum_scatter(jnp.dot(blended, output_weight, preferred_element_type=j...  86.7 us
    all_gather x1, blocking collectives, on_device(): portion = lax.all_gather(summaries, 'kv', axis=0, tiled=True)  35 us
    dot_general x2, matrix products, online_step(): jnp.einsum('grqk,kgd->grqd', weights.astype(jnp.bfloat16), values, prefer...  18.1 us
    dot_general x1, matrix products, span_step(): jnp.einsum('qgrd,kgd->grqk', queries, stretch[..., :HD], preferred_elemen...  15.2 us
    reduce_sum x2, other arithmetic, online_step(): summed = summed * shrink + jnp.sum(weights, -1)  15.2 us
    and x1, local copies, waits for them, and re-layouts, span_step(): listed & (key_positions[None, None, :] <= positions[None, :, None])  6.06 us
  transfers between devices with their start and end apart: 3, of which 1 were waited for; matrix products, arithmetic and copies ran while one was open for 14% of the time, Pallas kernels for 0%

commit v1 on v0

--- a/solution.py
+++ b/solution.py
@@ -130,7 +130,15 @@
         jnp.zeros((groups_here, per_group, tok_rows), jnp.float32),
         jnp.zeros((groups_here, per_group, tok_rows, HD), jnp.float32),
     )
-    portion = lax.all_gather(summaries, "kv", axis=0, tiled=True)
+    n_blocks = lax.axis_size("kv")
+    tall = [(no - 1, no) for no in range(1, n_blocks)] + [(n_blocks - 1, 0)]
+    state_now = summaries
+    log = [state_now]
+    for _ in [*range(n_blocks - 1)]:
+        state_now = lax.ppermute(state_now, axis_name="kv", perm=tall)
+        log += [state_now]
+    before = jnp.concatenate([*reversed(log)], axis=0)
+    portion = jnp.roll(before, shift=(lax.axis_index("kv") + 1) * state_now.shape[0], axis=0)
     length = portion.shape[0]
     ends = jnp.arange(length, dtype=jnp.int32) * CMP_STRIDE + CMP_LEN - 1
     scores = (

time: 242 us -> 245 us (1.012)
  waiting for transfers between devices: 86.8 us -> 124 us
  blocking collectives: 35 us -> 0 us
  starting transfers between devices: 1.32 us -> 5.1 us
    ppermute x0 -> x7, waiting for transfers between devices: none -> 40.5 us  [on_device(): state_now = lax.ppermute(state_now, axis_name='kv', perm=tall)]
    all_gather x1 -> x0, blocking collectives: 35 us -> none  [on_device(): portion = lax.all_gather(summaries, 'kv', axis=0, tiled=True)]
    ppermute x0 -> x7, starting transfers between devices: none -> 3.77 us  [on_device(): state_now = lax.ppermute(state_now, axis_name='kv', perm=tall)]
    reduce_scatter x1, waiting for transfers between devices: 86.7 us -> 83.2 us  [on_device(): lax.psum_scatter(jnp.dot(blended, output_weight, preferred_element_type=j...]
  transfers between devices with their start and end apart: 3 -> 10, of which waited for: 1 -> 8; matrix products, arithmetic and copies ran while one was open for 14% -> 13% of each run, Pallas kernels for 0% -> 0%
where the time goes in v1:
time: 245 us; the launch traced here: 244 us
  waiting for transfers between devices  124 us (51%)
  matrix products  60.5 us (25%)
  other arithmetic  24.7 us (10%)
  local copies, waits for them, and re-layouts  15.3 us (6%)
  between operations  13.9 us (6%)
  starting transfers between devices  5.1 us (2%)
    reduce_scatter x1, waiting for transfers between devices, on_device(): lax.psum_scatter(jnp.dot(blended, output_weight, preferred_element_type=j...  83.2 us
    ppermute x7, waiting for transfers between devices, on_device(): state_now = lax.ppermute(state_now, axis_name='kv', perm=tall)  40.5 us
    dot_general x2, matrix products, online_step(): jnp.einsum('grqk,kgd->grqd', weights.astype(jnp.bfloat16), values, prefer...  18.2 us
    dot_general x1, matrix products, span_step(): jnp.einsum('qgrd,kgd->grqk', queries, stretch[..., :HD], preferred_elemen...  15.2 us
    reduce_sum x2, other arithmetic, online_step(): summed = summed * shrink + jnp.sum(weights, -1)  15.2 us
    and x1, local copies, waits for them, and re-layouts, span_step(): listed & (key_positions[None, None, :] <= positions[None, :, None])  6.03 us
  transfers between devices with their start and end apart: 10, of which 8 were waited for; matrix products, arithmetic and copies ran while one was open for 13% of the time, Pallas kernels for 0%

profile of v1, /device:TPU:0, one launch (start us, length us, event | category | flops | bytes accessed | tf_op | source)
XLA Modules:
  0.0 243.6 jit_solution(2943875160501650842)
XLA Ops:
  6.6 2.7 %convolution_convert_fusion.1 = bf16[512,128]{0,1:T(8,128)(2,1)S(1)} fusion(bf16[512,2048]{1,0:T(8,128)(2,1)} %param.17, bf16[2048,128]{1,0:T(8,128)(2,1)} %param.20), kind=kOutput, calls=%fused_computation.44 | convolution fusion | flops 268500992 | bytes 2752512 | tf_op jit(solution)/shard_map/dot_general | solution.py:94
  9.2 2.5 %fusion.91 = f32[512,128]{0,1:T(8,128)S(1)} fusion(bf16[512,2048]{1,0:T(8,128)(2,1)} %param.17, bf16[2048,128]{1,0:T(8,128)(2,1)} %param.19), kind=kOutput, calls=%fused_computation.135 | convolution fusion | flops 268435456 | bytes 2883584 | tf_op jit(solution)/shard_map/dot_general | solution.py:88
  12.9 2.4 convolution_convert_fusion.2
  15.5 2.5 %convolution_convert_fusion.3 = bf16[512,128]{0,1:T(8,128)(2,1)S(1)} fusion(bf16[512,2048]{1,0:T(8,128)(2,1)} %param.17, bf16[2048,128]{1,0:T(8,128)(2,1)} %param.21), kind=kOutput, calls=%fused_computation.46 | convolution fusion | flops 268500992 | bytes 2752512 | tf_op jit(solution)/shard_map/dot_general | solution.py:100
  19.6 4.5 %fusion.90 = f32[512,512]{0,1:T(8,128)} fusion(bf16[512,2048]{1,0:T(8,128)(2,1)} %param.17, bf16[2048,512]{1,0:T(8,128)(2,1)} %param.18), kind=kOutput, calls=%fused_computation.134 | convolution fusion | flops 1073741824 | bytes 5242880 | tf_op jit(solution)/shard_map/dot_general | solution.py:81
  31.7 3.8 %collective-permute-start.1 = (bf16[32,2,128]{0,2,1:T(8,128)(2,1)S(1)}, bf16[32,2,128]{0,2,1:T(8,128)(2,1)S(1)}, u32[]{:S(2)}, u32[]{:S(2)}) collective-permute-start(bf16[32,2,128]{0,2,1:T(8,128)(2,1)S(1)} %pad_maximum_fusion.5), channel_id=1, source_target_pairs={{0,4},{4,8},{8,12},{12,16},{16,20},{20,24},{24,28},{28,0},{1,5},{5... | collective-permute-start | bytes 49160 | tf_op jit(solution)/shard_map/ppermute | solution.py:138
  37.7 3.9 %collective-permute-done.1 = bf16[32,2,128]{0,2,1:T(8,128)(2,1)S(1)} collective-permute-done((bf16[32,2,128]{0,2,1:T(8,128)(2,1)S(1)}, bf16[32,2,128]{0,2,1:T(8,128)(2,1)S(1)}, u32[]{:S(2)}, u32[]{:S(2)}) %collective-permute-start.1) | collective-permute-done | bytes 16416 | tf_op jit(solution)/shard_map/ppermute | solution.py:138
  41.6 2.9 %fusion.37 = f32[512,8]{0,1:T(8,128)} fusion(bf16[512,2048]{1,0:T(8,128)(2,1)} %param.17, bf16[2,2048,8]{1,2,0:T(8,128)(2,1)} %param.27), kind=kOutput, calls=%fused_computation.55 | convolution fusion | flops 16789504 | bytes 2146304 | tf_op jit(solution)/shard_map/dot_general | solution.py:192
  44.5 4.3 %collective-permute-done.2 = bf16[32,2,128]{0,2,1:T(8,128)(2,1)S(1)} collective-permute-done((bf16[32,2,128]{0,2,1:T(8,128)(2,1)S(1)}, bf16[32,2,128]{0,2,1:T(8,128)(2,1)S(1)}, u32[]{:S(2)}, u32[]{:S(2)}) %collective-permute-start.2) | collective-permute-done | bytes 16416 | tf_op jit(solution)/shard_map/ppermute | solution.py:138
  49.9 6.9 %collective-permute-done.3 = bf16[32,2,128]{0,2,1:T(8,128)(2,1)S(1)} collective-permute-done((bf16[32,2,128]{0,2,1:T(8,128)(2,1)S(1)}, bf16[32,2,128]{0,2,1:T(8,128)(2,1)S(1)}, u32[]{:S(2)}, u32[]{:S(2)}) %collective-permute-start.3) | collective-permute-done | bytes 16416 | tf_op jit(solution)/shard_map/ppermute | solution.py:138
  56.8 7.1 %collective-permute-done.4 = bf16[32,2,128]{0,2,1:T(8,128)(2,1)S(1)} collective-permute-done((bf16[32,2,128]{0,2,1:T(8,128)(2,1)S(1)}, bf16[32,2,128]{0,2,1:T(8,128)(2,1)S(1)}, u32[]{:S(2)}, u32[]{:S(2)}) %collective-permute-start.4) | collective-permute-done | bytes 16416 | tf_op jit(solution)/shard_map/ppermute | solution.py:138
  63.9 7.3 %collective-permute-done.5 = bf16[32,2,128]{0,2,1:T(8,128)(2,1)S(1)} collective-permute-done((bf16[32,2,128]{0,2,1:T(8,128)(2,1)S(1)}, bf16[32,2,128]{0,2,1:T(8,128)(2,1)S(1)}, u32[]{:S(2)}, u32[]{:S(2)}) %collective-permute-start.5) | collective-permute-done | bytes 16416 | tf_op jit(solution)/shard_map/ppermute | solution.py:138
  71.4 6.8 %collective-permute-done.6 = bf16[32,2,128]{0,2,1:T(8,128)(2,1)S(1)} collective-permute-done((bf16[32,2,128]{0,2,1:T(8,128)(2,1)S(1)}, bf16[32,2,128]{0,2,1:T(8,128)(2,1)S(1)}, u32[]{:S(2)}, u32[]{:S(2)}) %collective-permute-start.6) | collective-permute-done | bytes 16416 | tf_op jit(solution)/shard_map/ppermute | solution.py:138
  80.9 4.2 %collective-permute-done.7 = bf16[32,2,128]{0,2,1:T(8,128)(2,1)S(1)} collective-permute-done((bf16[32,2,128]{0,2,1:T(8,128)(2,1)S(1)}, bf16[32,2,128]{0,2,1:T(8,128)(2,1)S(1)}, u32[]{:S(2)}, u32[]{:S(2)}) %collective-permute-start.7) | collective-permute-done | bytes 16416 | tf_op jit(solution)/shard_map/ppermute | solution.py:138
  92.3 55.1 %while.20 = (s32[]{:T(128)}, f32[2,4,512]{2,1,0:T(4,128)S(1)}, f32[2,4,512]{2,1,0:T(4,128)S(1)}, f32[2,4,512,64]{2,3,1,0:T(8,128)S(1)}, s32[]{:T(128)}, /*index=...) while((s32[]{:T(128)}, f32[2,4,512]{2,1,0:T(4,128)S(1)}, ...), condition=%wide.region_8.9_spmd.clone, body=%wide.region_2.8_spmd.clone.sunk | while | flops 2245501440 | bytes 127838584 | solution.py:189
  92.5 54.8 %conditional.3 = ((f32[2,4,512]{2,1,0:T(4,128)S(1)}, f32[2,4,512]{2,1,0:T(4,128)S(1)}, f32[2,4,512,64]{2,3,1,0:T(8,128)S(1)})) conditional(s32[]{:T(128)} %convert_element_type.107, (f32[2,4,512]{2,1,0:T(4,128)S(1)}, f32[2,4,512]{2,1,0:T(4,128)S(1)}, f32[2,4,512,64]{2,3,1,0:T(8,128)S(1)}) %tuple.69, (s32[2,16,16]{2,1,0:T(8,128)S(1)}, s32[]{:T(128)}, ...), branch_computations={%region_3.3_spmd, %region_4.7_spmd} | conditional | flops 2245501440 | bytes 127836296 | solution.py:179
  94.3 2.6 %bitcast_and_fusion = pred[2,512,2048]{2,1,0:T(8,128)(4,1)} fusion(pred[512,2048]{1,0:T(8,128)(4,1)S(1)} %broadcast_compare_fusion, pred[2,16,2048]{2,1,0:T(8,128)(4,1)S(1)} %compare_reduce_fusion), kind=kLoop, calls=%fused_computation.10 | loop fusion | flops 2097152 | bytes 3211264 | tf_op jit(solution)/shard_map/while/body/eval_jaxpr/cond/branch_1_fun/and | solution.py:162
  96.9 6.0 %copy.48 = pred[2,512,2048]{1,2,0:T(8,128)(4,1)} copy(pred[2,512,2048]{2,1,0:T(8,128)(4,1)} %bitcast_and_fusion) | data formatting | bytes 4194304 | tf_op jit(solution)/shard_map/while/body/eval_jaxpr/cond/branch_1_fun/and | solution.py:162
  103.0 15.2 %fusion.2 = (f32[2,4,512]{2,1,0:T(4,128)S(1)}, f32[2,2048,512,4]{2,1,3,0:T(8,128)}) fusion(pred[2,512,2048]{1,2,0:T(8,128)(4,1)} %copy.48, bf16[512,2,4,64]{0,3,2,1:T(8,128)(2,1)} %get-tuple-element.301, bf16[4096,2,128]{0,2,1:T(8,128)(2,1)} %get-tuple-element.300, s32[]{:T(128)S(6)} %select_n.46), kind=kOutput, calls=%fused_computation.3 | convolution fusion | flops 1098903552 | bytes 36716548 | tf_op jit(solution)/shard_map/while/body/eval_jaxpr/cond/branch_1_fun/qgrd,kgd->grqk/dot_general | solution.py:164
  118.2 14.3 %fusion.6 = f32[2,4,512]{2,1,0:T(4,128)S(1)} fusion(f32[2,2048,512,4]{2,1,3,0:T(8,128)} %get-tuple-element.369, f32[2,4,512]{2,1,0:T(4,128)S(1)} %max.12, pred[2,512,2048]{1,2,0:T(8,128)(4,1)S(1)} %copy-done.1), kind=kLoop, calls=%fused_computation.7 | loop fusion | flops 33550336 | bytes 35684352 | tf_op jit(solution)/shard_map/while/body/eval_jaxpr/cond/branch_1_fun/reduce_sum | solution.py:51
  132.6 14.8 %fusion.10 = f32[2,4,512,64]{2,3,1,0:T(8,128)S(1)} fusion(f32[2,2048,512,4]{2,1,3,0:T(8,128)} %get-tuple-element.369, f32[2,4,512]{2,1,0:T(4,128)S(1)} %max.12, pred[2,512,2048]{1,2,0:T(8,128)(4,1)} %copy.48, f32[2,4,512,64]{2,3,1,0:T(8,128)S(1)} %get-tuple-element.303, bf16[4096,2,128]{0,2,1:T(8,128)(2,1)} %get-tuple-element.300, s32[]{:T(128)S(6)} %select_n.46, ...), kind=kOutput, calls=%fused_computation.13 | convolution fusion | flops 1107820544 | bytes 38305800 | tf_op jit(solution)/shard_map/while/body/eval_jaxpr/cond/branch_1_fun/grqk,kgd->grqd/dot_general | solution.py:52
  147.5 3.4 %add_convert_fusion = bf16[2,4,512,64]{2,3,1,0:T(8,128)(2,1)S(1)} fusion(f32[2,4,512,64]{2,3,1,0:T(8,128)S(1)} %get-tuple-element.319, f32[2,256,512,4]{2,1,3,0:T(8,128)} %copy-done.2, f32[2,4,512]{2,1,0:T(4,128)S(1)} %copy-done.15, pred[512,256]{0,1:T(8,128)(4,1)S(1)} %copy-done.7, f32[2,4,512]{2,1,0:T(4,128)S(1)} %get-tuple-element.320, ...), kind=kOutput, calls=%fused_computation.56 | convolution fusion | flops 140247040 | bytes 6062088 | tf_op jit(solution)/shard_map/grqk,kgd->grqd/dot_general | solution.py:52
  150.9 2.6 %convolution_convert_fusion = bf16[512,2048]{1,0:T(8,128)(2,1)} fusion(bf16[512,512]{0,1:T(8,128)(2,1)S(1)} %bitcast.140, bf16[512,2048]{1,0:T(8,128)(2,1)S(1)} %copy-done), kind=kOutput, calls=%fused_computation.40 | convolution fusion | flops 1074790400 | bytes 4718592 | tf_op jit(solution)/shard_map/dot_general | solution.py:210
  153.5 83.2 %reduce-scatter.2.cloned.1.call-done = bf16[128,2048]{1,0:T(8,128)(2,1)} async-done(((bf16[512,2048]{1,0:T(8,128)(2,1)}), bf16[128,2048]{1,0:T(8,128)(2,1)}) %reduce-scatter.2.cloned.1.call-update) | async-done | bytes 524304 | tf_op jit(solution)/shard_map/reduce_scatter | solution.py:209
  (113 shorter events, 25.4 us)
Async XLA Ops:
  6.5 144.3 %copy-start = (bf16[512,2048]{1,0:T(8,128)(2,1)S(1)}, bf16[512,2048]{1,0:T(8,128)(2,1)}, u32[]{:S(2)}) copy-start(bf16[512,2048]{1,0:T(8,128)(2,1)} %param.28) | copy-start | bytes 6291460
  6.5 85.6 %all-gather.2.cloned.1.call-start = ((), (), s32[]{:S(2)}) async-start(), calls=%async_computation.1 | async-start | bytes 2359296 | tf_op jit(solution)/shard_map/all_gather | solution.py:181
  12.9 223.9 %reduce-scatter.2.cloned.1.call-start = ((), (), s32[]{:S(2)}) async-start(), calls=%async_computation.2 | async-start | bytes 2621440 | tf_op jit(solution)/shard_map/reduce_scatter | solution.py:209
  18.3 6.5 %collective-permute-start = (bf16[16,2,128]{2,0,1:T(8,128)(2,1)S(1)}, bf16[16,2,128]{2,0,1:T(8,128)(2,1)S(1)}, u32[]{:S(2)}, u32[]{:S(2)}) collective-permute-start(bf16[16,2,128]{2,0,1:T(8,128)(2,1)S(1)} %pad_maximum_fusion.6), channel_id=1, source_target_pairs={{4,0},{8,4},{12,8},{16,12},{20,16},{24,20},{28,24},{5,1},{9,5},{13... | collective-permute-start | bytes 24584 | tf_op jit(solution)/shard_map/ppermute | solution.py:17
  31.3 17.5 %copy-start.3 = (f32[512,512]{0,1:T(8,128)S(1)}, f32[512,512]{0,1:T(8,128)}, u32[]{:S(2)}) copy-start(f32[512,512]{0,1:T(8,128)} %fusion.90) | copy-start | bytes 3145732
  31.7 10.0 %collective-permute-start.1 = (bf16[32,2,128]{0,2,1:T(8,128)(2,1)S(1)}, bf16[32,2,128]{0,2,1:T(8,128)(2,1)S(1)}, u32[]{:S(2)}, u32[]{:S(2)}) collective-permute-start(bf16[32,2,128]{0,2,1:T(8,128)(2,1)S(1)} %pad_maximum_fusion.5), channel_id=1, source_target_pairs={{0,4},{4,8},{8,12},{12,16},{16,20},{20,24},{24,28},{28,0},{1,5},{5... | collective-permute-start | bytes 49160 | tf_op jit(solution)/shard_map/ppermute | solution.py:138
  41.6 7.2 %copy-start.11 = (bf16[32,2,128]{0,2,1:T(8,128)(2,1)}, bf16[32,2,128]{0,2,1:T(8,128)(2,1)S(1)}, u32[]{:S(2)}) copy-start(bf16[32,2,128]{0,2,1:T(8,128)(2,1)S(1)} %collective-permute-done.1) | copy-start | bytes 49156
  41.6 7.2 %collective-permute-start.2 = (bf16[32,2,128]{0,2,1:T(8,128)(2,1)S(1)}, bf16[32,2,128]{0,2,1:T(8,128)(2,1)S(1)}, u32[]{:S(2)}, u32[]{:S(2)}) collective-permute-start(bf16[32,2,128]{0,2,1:T(8,128)(2,1)S(1)} %collective-permute-done.1), channel_id=1, source_target_pairs={{0,4},{4,8},{8,12},{12,16},{16,20},{20,24},{24,28},{28,0},{1,5},{5... | collective-permute-start | bytes 49160 | tf_op jit(solution)/shard_map/ppermute | solution.py:138
  48.8 22.4 %copy-start.12 = (bf16[32,2,128]{0,2,1:T(8,128)(2,1)}, bf16[32,2,128]{0,2,1:T(8,128)(2,1)S(1)}, u32[]{:S(2)}) copy-start(bf16[32,2,128]{0,2,1:T(8,128)(2,1)S(1)} %collective-permute-done.2) | copy-start | bytes 49156
  48.8 8.0 %collective-permute-start.3 = (bf16[32,2,128]{0,2,1:T(8,128)(2,1)S(1)}, bf16[32,2,128]{0,2,1:T(8,128)(2,1)S(1)}, u32[]{:S(2)}, u32[]{:S(2)}) collective-permute-start(bf16[32,2,128]{0,2,1:T(8,128)(2,1)S(1)} %collective-permute-done.2), channel_id=1, source_target_pairs={{0,4},{4,8},{8,12},{12,16},{16,20},{20,24},{24,28},{28,0},{1,5},{5... | collective-permute-start | bytes 49160 | tf_op jit(solution)/shard_map/ppermute | solution.py:138
  49.8 28.3 %copy-start.4 = (bf16[512,8,32]{0,2,1:T(8,128)(2,1)}, bf16[512,8,32]{0,2,1:T(8,128)(2,1)S(1)}, u32[]{:S(2)}) copy-start(bf16[512,8,32]{0,2,1:T(8,128)(2,1)S(1)} %get-tuple-element.373) | copy-start | bytes 786436
  56.8 14.4 %copy-start.13 = (bf16[32,2,128]{0,2,1:T(8,128)(2,1)}, bf16[32,2,128]{0,2,1:T(8,128)(2,1)S(1)}, u32[]{:S(2)}) copy-start(bf16[32,2,128]{0,2,1:T(8,128)(2,1)S(1)} %collective-permute-done.3) | copy-start | bytes 49156
  56.8 7.1 %collective-permute-start.4 = (bf16[32,2,128]{0,2,1:T(8,128)(2,1)S(1)}, bf16[32,2,128]{0,2,1:T(8,128)(2,1)S(1)}, u32[]{:S(2)}, u32[]{:S(2)}) collective-permute-start(bf16[32,2,128]{0,2,1:T(8,128)(2,1)S(1)} %collective-permute-done.3), channel_id=1, source_target_pairs={{0,4},{4,8},{8,12},{12,16},{16,20},{20,24},{24,28},{28,0},{1,5},{5... | collective-permute-start | bytes 49160 | tf_op jit(solution)/shard_map/ppermute | solution.py:138
  63.9 7.3 %collective-permute-start.5 = (bf16[32,2,128]{0,2,1:T(8,128)(2,1)S(1)}, bf16[32,2,128]{0,2,1:T(8,128)(2,1)S(1)}, u32[]{:S(2)}, u32[]{:S(2)}) collective-permute-start(bf16[32,2,128]{0,2,1:T(8,128)(2,1)S(1)} %collective-permute-done.4), channel_id=1, source_target_pairs={{0,4},{4,8},{8,12},{12,16},{16,20},{20,24},{24,28},{28,0},{1,5},{5... | collective-permute-start | bytes 49160 | tf_op jit(solution)/shard_map/ppermute | solution.py:138
  71.2 7.0 %collective-permute-start.6 = (bf16[32,2,128]{0,2,1:T(8,128)(2,1)S(1)}, bf16[32,2,128]{0,2,1:T(8,128)(2,1)S(1)}, u32[]{:S(2)}, u32[]{:S(2)}) collective-permute-start(bf16[32,2,128]{0,2,1:T(8,128)(2,1)S(1)} %collective-permute-done.5), channel_id=1, source_target_pairs={{0,4},{4,8},{8,12},{12,16},{16,20},{20,24},{24,28},{28,0},{1,5},{5... | collective-permute-start | bytes 49160 | tf_op jit(solution)/shard_map/ppermute | solution.py:138
  71.3 20.1 %copy-start.6 = (pred[512,256]{0,1:T(8,128)(4,1)}, pred[512,256]{0,1:T(8,128)(4,1)S(1)}, u32[]{:S(2)}) copy-start(pred[512,256]{0,1:T(8,128)(4,1)S(1)} %broadcast_compare_fusion.1) | copy-start | bytes 393220
  78.2 7.0 %collective-permute-start.7 = (bf16[32,2,128]{0,2,1:T(8,128)(2,1)S(1)}, bf16[32,2,128]{0,2,1:T(8,128)(2,1)S(1)}, u32[]{:S(2)}, u32[]{:S(2)}) collective-permute-start(bf16[32,2,128]{0,2,1:T(8,128)(2,1)S(1)} %collective-permute-done.6), channel_id=1, source_target_pairs={{0,4},{4,8},{8,12},{12,16},{16,20},{20,24},{24,28},{28,0},{1,5},{5... | collective-permute-start | bytes 49160 | tf_op jit(solution)/shard_map/ppermute | solution.py:138
  92.3 55.2 %copy-start.7 = (pred[512,256]{0,1:T(8,128)(4,1)S(1)}, pred[512,256]{0,1:T(8,128)(4,1)}, u32[]{:S(2)}) copy-start(pred[512,256]{0,1:T(8,128)(4,1)} %copy-done.6) | copy-start | bytes 393220
  92.3 55.2 %copy-start.15 = (f32[2,4,512]{2,1,0:T(4,128)S(1)}, f32[2,4,512]{2,1,0:T(4,128)}, u32[]{:S(2)}) copy-start(f32[2,4,512]{2,1,0:T(4,128)} %copy-done.14) | copy-start | bytes 49156
  92.3 55.2 %copy-start.18 = (f32[512,2,4]{0,2,1:T(4,128)S(1)}, f32[512,2,4]{0,2,1:T(4,128)}, u32[]{:S(2)}) copy-start(f32[512,2,4]{0,2,1:T(4,128)} %reshape.285) | copy-start | bytes 49156
  92.3 55.2 %copy-start.19 = (f32[512,2,4]{0,2,1:T(4,128)S(1)}, f32[512,2,4]{0,2,1:T(4,128)}, u32[]{:S(2)}) copy-start(f32[512,2,4]{0,2,1:T(4,128)} %reshape.278) | copy-start | bytes 49156
  92.3 55.2 %copy-start.20 = (f32[2,4,512]{2,1,0:T(4,128)S(1)}, f32[2,4,512]{2,1,0:T(4,128)}, u32[]{:S(2)}) copy-start(f32[2,4,512]{2,1,0:T(4,128)} %get-tuple-element.382) | copy-start | bytes 49156
  92.3 55.2 %copy-start.21 = (f32[2,4,512]{2,1,0:T(4,128)S(1)}, f32[2,4,512]{2,1,0:T(4,128)}, u32[]{:S(2)}) copy-start(f32[2,4,512]{2,1,0:T(4,128)} %get-tuple-element.383) | copy-start | bytes 49156
  103.0 15.2 %copy-start.1 = (pred[2,512,2048]{1,2,0:T(8,128)(4,1)S(1)}, pred[2,512,2048]{1,2,0:T(8,128)(4,1)}, u32[]{:S(2)}) copy-start(pred[2,512,2048]{1,2,0:T(8,128)(4,1)} %copy.48) | copy-start | bytes 6291460 | tf_op jit(solution)/shard_map/while/body/eval_jaxpr/cond
  (8 other events, 37.4 us)
Sparse Core Ops, SparseCore 0:
  13.0 56.1 all-gather.1
  153.6 83.0 reduce-scatter.1
